TPU v7x, 512 devices: a whole 4x4x16 slice. The times are simulated.
512 devices in a mesh: vp: 128 (over z, x, core), dp: 4 (over y).
Axes of the slice: x: 4, y: 4, z: 16, core: 2. Of those that a mesh axis runs over, the one named last changes fastest.
Arguments:
- stream: bfloat16 [1024, 2048], P(('dp', 'vp')), may hold values from -60 to 60
- hidden: bfloat16 [1024, 5632], P('dp', 'vp'), may hold values from -6 to 6
- w_down: bfloat16 [5632, 2048], P(None, 'vp'), may hold values from -0.078125 to 0.078125
- final_gain: float32 [2048], replicated, may hold values from 0.1 to 1.9
- vocab: bfloat16 [2048, 32768], P(None, 'vp'), may hold values from -2 to 200
- vocab_bias: float32 [32768], P('vp'), may hold values from -5 to 5
- targets: int32 [1024], P('dp'), may hold values from 0 to 32767
Outputs:
- losses: float32 [1024], P(('dp', 'vp'))
- grad_input: float32 [1024, 2048], P(('dp', 'vp'))
- grad_vocab: float32 [2048, 32768], P('dp', 'vp')
All inputs are finite; a program needn't handle non-finite values.
Results may differ from a plain program's by a relative error of at most 0.02.
Values may be sent and summed in bfloat16 or wider, within the bound.
No kernel may reach another device: no remote copies, remote signals or barrier semaphores. Data moves between devices by JAX's collectives and lax.ppermute only.
A program may use at most 64 MiB of HBM per device.

v0:
```python
import jax
import jax.numpy as jnp
import numpy as np
from jax import lax
from jax.sharding import Mesh
from jax.sharding import PartitionSpec as P


Z, X, C = "vp_0", "vp_1", "vp_2"
Q = ("vp_1", "vp_2")
ZX = ("vp_0", "vp_1")
VP = ("vp_0", "vp_1", "vp_2")
DP_VP = ("dp", "vp_0", "vp_1", "vp_2")

norm_eps = 1e-06
zloss_weight = 0.001
f32 = jnp.float32
bf16 = jnp.bfloat16


def exchange(blocks, axes):
    return lax.all_to_all(blocks, axes, split_axis=0, concat_axis=0, tiled=True)


def shared(block, axes, count):
    return exchange(jnp.broadcast_to(block[None], (count, *block.shape)), axes)


def partner(array, axes, step):
    return lax.ppermute(array, axes, [(k, k ^ step) for k in range(lax.axis_size(axes))])


def dot(a, b, da, db):
    return lax.dot_general(a, b, (((da,), (db,)), ((), ())), preferred_element_type=f32)


def blocks_over_x(rows, x, span):
    blocks = [lax.dynamic_slice_in_dim(rows, (x ^ k) * span, span) for k in range(rows.shape[0] // span)]
    return [partner(b, X, k) if k else b for k, b in enumerate(blocks)]


def halves(array, core):
    first = lax.dynamic_slice_in_dim(array, core * (array.shape[0] // 2), array.shape[0] // 2)
    other = (1 - core) * (array.shape[0] // 2)
    return first, lax.dynamic_slice_in_dim(array, other, array.shape[0] // 2)


def body(stream, hidden, w_down, final_gain, vocab, vocab_bias, targets):
    nz, nx, nc, ny = (lax.axis_size(a) for a in (Z, X, C, "dp"))
    z, x, c, y = (lax.axis_index(a) for a in (Z, X, C, "dp"))
    nq = nx * nc
    own, width = stream.shape
    group, units = hidden.shape
    cols = w_down.shape[1]
    ncols = vocab.shape[1]
    mine = (z * nx + x) * nc + c
    span = nz * own
    half = nx * span
    feats = nq * cols
    rows = -(-(units + own) // 16) * 16

    order = np.arange(group).reshape(nz, nq, own).transpose(1, 0, 2).reshape(-1)
    order = jnp.asarray(np.eye(group, dtype=np.float32)[order], bf16)
    mine_h = dot(hidden, order, 0, 1).astype(bf16)
    part = stream.reshape(own, nz, feats).transpose(1, 0, 2)
    part = jnp.pad(part, ((0, 0), (units, rows - units - own), (0, group - feats)))
    mine_h = jnp.pad(mine_h, ((0, rows - units), (0, 0)))
    first = exchange(mine_h[None] + part, Z)

    blocks = w_down.T.reshape(cols, nz, nq, units).transpose(2, 0, 1, 3)
    blocks = jnp.pad(blocks, ((0, 0), (0, 0), (0, 0), (0, rows - units)))
    blocks = blocks.reshape(nx, nc, cols, nz * rows).transpose(1, 0, 2, 3)
    kept, sent = halves(blocks, c)
    came = partner(sent, C, 1)
    pair = jnp.concatenate([jnp.where(c == 0, kept, came), jnp.where(c == 0, came, kept)], axis=0)
    pair = pair.transpose(1, 0, 2, 3)
    w_rows = jnp.zeros_like(pair)
    for step in range(nx):
        block = lax.dynamic_slice_in_dim(pair, x ^ step, 1)
        block = partner(block, X, step) if step else block
        w_rows = lax.dynamic_update_slice_in_dim(w_rows, block, x ^ step, 0)

    partial = dot(first.reshape(nz * rows, group), w_rows.reshape(feats, nz * rows), 0, 1)

    vocab, vocab_bias, partial = lax.optimization_barrier((vocab, vocab_bias, partial))
    vocab = (vocab, partner(vocab, C, 1))
    bias = (vocab_bias, partner(vocab_bias.reshape(2, -1), C, 1).reshape(-1))
    line = lax.broadcasted_iota(jnp.int32, (half, group), 0)
    token = (line // own) % nz * (nq * own) + line // span * (nc * own) + c * own + line % own
    goals = jnp.where(token == lax.broadcasted_iota(jnp.int32, (half, group), 1), targets[None, :], 0)
    goals = jnp.sum(goals, axis=1)
    ids = lax.broadcasted_iota(jnp.int32, (half, ncols), 1)
    hit = [ids + k * ncols == goals[:, None] for k in (mine, mine ^ 1)]

    proj = jnp.sum(exchange(partial.reshape(nq, span, feats), Q), axis=0)
    row_part = first[:, units : units + own, :feats].reshape(span, feats)
    normin = (row_part.astype(f32) + proj).astype(bf16)
    goal_rows = sum(dot(h.astype(bf16), v, 1, 1) for h, v in zip(hit, vocab)).astype(bf16)
    goal_rows = blocks_over_x(goal_rows, x, span)
    normin, *goal_rows = lax.optimization_barrier((shared(normin, Z, nz), *goal_rows))
    goal_rows = sum(g.astype(f32) for g in goal_rows)
    normin = normin.transpose(1, 0, 2).reshape(span, width)
    values = normin.astype(f32)
    inv = lax.rsqrt(jnp.mean(values * values, axis=1, keepdims=True) + norm_eps)
    normed = (values * inv * final_gain).astype(bf16)
    normed = shared(normed, X, nx).reshape(half, width)

    scores = [dot(normed, v, 1, 0) + b for v, b in zip(vocab, bias)]
    top = jnp.maximum(jnp.max(scores[0], axis=1), jnp.max(scores[1], axis=1))
    total = sum(jnp.sum(jnp.exp(s - top[:, None]), axis=1) for s in scores)
    goal = sum(jnp.sum(jnp.where(h, s, 0.0), axis=1) for h, s in zip(hit, scores))
    local = top + jnp.log(total)
    stats = shared(jnp.stack([local, goal]), ZX, nz * nx)
    terms = sum(
        dot(jnp.where(h, 0.0, jnp.exp(s - local[:, None])).astype(bf16), v, 1, 1)
        for h, s, v in zip(hit, scores, vocab)
    ).astype(bf16)
    terms = blocks_over_x(terms, x, span)

    top = jnp.max(stats[:, 0], axis=0)
    lse = top + jnp.log(jnp.sum(jnp.exp(stats[:, 0] - top), axis=0))
    goal = jnp.sum(stats[:, 1], axis=0)
    losses = lse - goal + zloss_weight * lse * lse
    losses = lax.dynamic_slice_in_dim(losses, x * span + z * own, own)
    scale = 1.0 + 2.0 * zloss_weight * lse
    dscore = [
        (jnp.exp(s - lse[:, None]) * scale[:, None] - jnp.where(h, 1.0, 0.0)).astype(bf16)
        for s, h in zip(scores, hit)
    ]
    shares = jnp.concatenate([jnp.exp(stats[:, 0] - lse) * scale, (jnp.exp(goal - lse) * scale - 1.0)[None]])
    shares = lax.dynamic_slice_in_dim(shares, x * span, span, 1)
    row_x = shares[-1][:, None] * goal_rows
    for step in range(nx):
        share = lax.dynamic_slice_in_dim(shares, z * nx + (x ^ step), 1)
        row_x = row_x + share.reshape(span, 1) * terms[step].astype(f32)
    row_x = row_x.astype(bf16)

    row_x, *dscore = lax.optimization_barrier((row_x, *dscore))
    feat_group = width // ny
    pieces = []
    for step in range(ny):
        piece = lax.dynamic_slice_in_dim(normed, (y ^ step) * feat_group, feat_group, 1)
        piece = jnp.concatenate([piece, *dscore], axis=1)
        pieces.append(partner(piece, "dp", step) if step else piece)
    pieces = jnp.concatenate(pieces)
    at = feat_group + ncols
    theirs = dot(pieces[:, :feat_group], pieces[:, at:], 0, 0)
    grad_vocab = dot(pieces[:, :feat_group], pieces[:, feat_group:at], 0, 0) + partner(theirs, C, 1)

    row_z = exchange(row_x.reshape(nz, own, width), Z)
    dnormed = jnp.sum(row_z.astype(f32), axis=0)

    values = lax.dynamic_slice_in_dim(values, z * own, own)
    inv = lax.dynamic_slice_in_dim(inv, z * own, own)
    scaled = dnormed * final_gain
    grad_input = inv * (
        scaled - values * inv * inv * jnp.mean(values * scaled, axis=1, keepdims=True)
    )
    return (losses, grad_input, grad_vocab)


def solution(mesh):
    torus = Mesh(mesh.devices.reshape(16, 4, 2, mesh.shape["dp"]), ("vp_0", "vp_1", "vp_2", "dp"))
    return jax.shard_map(
        body,
        mesh=torus,
        in_specs=(P(DP_VP, None), P("dp", VP), P(None, VP), P(), P(None, VP), P(VP), P("dp")),
        out_specs=(P(DP_VP), P(DP_VP, None), P("dp", VP)),
        check_vma=False,
    )
```

profile of v0, /device:TPU:24, one launch (start us, length us, event | category | flops | bytes accessed | tf_op | source)
XLA Modules:
  0.0 167.9 jit_solution(437242845192389949)
XLA Ops:
  3.9 15.2 %all-to-all-start = ((bf16[16,48,256]{2,1,0:T(8,128)(2,1)}), bf16[16,48,256]{2,1,0:T(8,128)(2,1)S(1)}, u32[]{:S(2)}, u32[]{:S(2)}) async-start(bf16[16,48,256]{2,1,0:T(8,128)(2,1)} %pad_add_fusion), calls=%async_computation | async-start | bytes 786432 | tf_op jit(solution)/shard_map/all_to_all | solution.py:22
  19.2 1.5 reshape.258
  21.3 1.9 %collective-permute-start = (bf16[1,4,16,768]{3,2,1,0:T(8,128)(2,1)S(1)}, bf16[1,4,16,768]{3,2,1,0:T(8,128)(2,1)S(1)}, u32[]{:S(2)}, u32[]{:S(2)}) collective-permute-start(bf16[1,4,16,768]{3,2,1,0:T(8,128)(2,1)S(1)} %dynamic-slice_bitcast_fusion), channel_id=1, source_target_pairs={{0,4},{4,0},{1,5},{5,1},{2,6},{6,2},{3,7},{7,3},{8,12},{12,8},{9,1... | collective-permute-start | bytes 294920 | tf_op jit(solution)/shard_map/ppermute | solution.py:30
  24.6 3.4 %collective-permute-start.1 = (bf16[1,2,16,768]{3,2,1,0:T(8,128)(2,1)S(1)}, bf16[1,2,16,768]{3,2,1,0:T(8,128)(2,1)S(1)}, u32[]{:S(2)}, u32[]{:S(2)}) collective-permute-start(bf16[1,2,16,768]{3,2,1,0:T(8,128)(2,1)S(1)} %get-tuple-element.49), channel_id=1, source_target_pairs={{0,8},{8,0},{16,24},{24,16},{1,9},{9,1},{17,25},{25,17},{2,10},{10... | collective-permute-start | bytes 147464 | tf_op jit(solution)/shard_map/ppermute | solution.py:30
  28.0 4.6 %collective-permute-start.2 = (bf16[1,2,16,768]{3,2,1,0:T(8,128)(2,1)S(1)}, bf16[1,2,16,768]{3,2,1,0:T(8,128)(2,1)S(1)}, u32[]{:S(2)}, u32[]{:S(2)}) collective-permute-start(bf16[1,2,16,768]{3,2,1,0:T(8,128)(2,1)S(1)} %get-tuple-element.50), channel_id=1, source_target_pairs={{0,16},{8,24},{16,0},{24,8},{1,17},{9,25},{17,1},{25,9},{2,18},{10... | collective-permute-start | bytes 147464 | tf_op jit(solution)/shard_map/ppermute | solution.py:30
  32.7 2.4 %collective-permute-start.3 = (bf16[1,2,16,768]{3,2,1,0:T(8,128)(2,1)S(1)}, bf16[1,2,16,768]{3,2,1,0:T(8,128)(2,1)S(1)}, u32[]{:S(2)}, u32[]{:S(2)}) collective-permute-start(bf16[1,2,16,768]{3,2,1,0:T(8,128)(2,1)S(1)} %get-tuple-element.48), channel_id=1, source_target_pairs={{0,24},{8,16},{16,8},{24,0},{1,25},{9,17},{17,9},{25,1},{2,26},{10... | collective-permute-start | bytes 147464 | tf_op jit(solution)/shard_map/ppermute | solution.py:30
  35.5 4.3 %collective-permute-done.3 = bf16[1,2,16,768]{3,2,1,0:T(8,128)(2,1)S(1)} collective-permute-done((bf16[1,2,16,768]{3,2,1,0:T(8,128)(2,1)S(1)}, bf16[1,2,16,768]{3,2,1,0:T(8,128)(2,1)S(1)}, u32[]{:S(2)}, u32[]{:S(2)}) %collective-permute-start.3) | collective-permute-done | bytes 49184 | tf_op jit(solution)/shard_map/ppermute | solution.py:30
  39.9 3.1 %all-to-all-done = bf16[16,48,256]{2,1,0:T(8,128)(2,1)S(1)} async-done(((bf16[16,48,256]{2,1,0:T(8,128)(2,1)}), bf16[16,48,256]{2,1,0:T(8,128)(2,1)S(1)}, u32[]{:S(2)}, u32[]{:S(2)}) %all-to-all-start) | async-done | bytes 393248 | tf_op jit(solution)/shard_map/all_to_all | solution.py:22
  44.7 1.9 %collective-permute-start.4 = (bf16[2048,256]{1,0:T(8,128)(2,1)S(1)}, bf16[2048,256]{1,0:T(8,128)(2,1)S(1)}, u32[]{:S(2)}, u32[]{:S(2)}) collective-permute-start(bf16[2048,256]{1,0:T(8,128)(2,1)S(1)} %copy-done.1), channel_id=1, source_target_pairs={{0,4},{4,0},{1,5},{5,1},{2,6},{6,2},{3,7},{7,3},{8,12},{12,8},{9,1... | collective-permute-start | bytes 3145736 | tf_op jit(solution)/shard_map/ppermute | solution.py:30
  46.9 4.4 %all-to-all-start.1 = ((f32[8,32,128]{2,1,0:T(8,128)}), f32[8,32,128]{2,1,0:T(8,128)S(1)}, u32[]{:S(2)}, u32[]{:S(2)}) async-start(f32[8,32,128]{2,1,0:T(8,128)} %bitcast.14), calls=%async_computation.1 | async-start | bytes 262144 | tf_op jit(solution)/shard_map/all_to_all | solution.py:22
  52.6 4.8 %all-to-all-done.1 = f32[8,32,128]{2,1,0:T(8,128)S(1)} async-done(((f32[8,32,128]{2,1,0:T(8,128)}), f32[8,32,128]{2,1,0:T(8,128)S(1)}, u32[]{:S(2)}, u32[]{:S(2)}) %all-to-all-start.1) | async-done | bytes 131104 | tf_op jit(solution)/shard_map/all_to_all | solution.py:22
  58.1 7.8 %all-to-all-start.2 = ((bf16[16,32,128]{2,1,0:T(8,128)(2,1)}), bf16[16,32,128]{2,1,0:T(8,128)(2,1)S(1)}, u32[]{:S(2)}, u32[]{:S(2)}) async-start(bf16[16,32,128]{2,1,0:T(8,128)(2,1)} %broadcast_in_dim.32), calls=%async_computation.2 | async-start | bytes 262144 | tf_op jit(solution)/shard_map/all_to_all | solution.py:22
  66.6 2.5 %collective-permute-start.5 = (bf16[32,2048]{1,0:T(8,128)(2,1)S(1)}, bf16[32,2048]{1,0:T(8,128)(2,1)S(1)}, u32[]{:S(2)}, u32[]{:S(2)}) collective-permute-start(bf16[32,2048]{1,0:T(8,128)(2,1)S(1)} %get-tuple-element.44), channel_id=1, source_target_pairs={{0,8},{8,0},{16,24},{24,16},{1,9},{9,1},{17,25},{25,17},{2,10},{10... | collective-permute-start | bytes 393224 | tf_op jit(solution)/shard_map/ppermute | solution.py:30
  69.0 4.0 %collective-permute-start.6 = (bf16[32,2048]{1,0:T(8,128)(2,1)S(1)}, bf16[32,2048]{1,0:T(8,128)(2,1)S(1)}, u32[]{:S(2)}, u32[]{:S(2)}) collective-permute-start(bf16[32,2048]{1,0:T(8,128)(2,1)S(1)} %get-tuple-element.43), channel_id=1, source_target_pairs={{0,16},{8,24},{16,0},{24,8},{1,17},{9,25},{17,1},{25,9},{2,18},{10... | collective-permute-start | bytes 393224 | tf_op jit(solution)/shard_map/ppermute | solution.py:30
  73.0 4.0 %collective-permute-start.7 = (bf16[32,2048]{1,0:T(8,128)(2,1)S(1)}, bf16[32,2048]{1,0:T(8,128)(2,1)S(1)}, u32[]{:S(2)}, u32[]{:S(2)}) collective-permute-start(bf16[32,2048]{1,0:T(8,128)(2,1)S(1)} %get-tuple-element.42), channel_id=1, source_target_pairs={{0,24},{8,16},{16,8},{24,0},{1,25},{9,17},{17,9},{25,1},{2,26},{10... | collective-permute-start | bytes 393224 | tf_op jit(solution)/shard_map/ppermute | solution.py:30
  77.0 3.5 %all-to-all-done.2 = bf16[16,32,128]{2,1,0:T(8,128)(2,1)S(1)} async-done(((bf16[16,32,128]{2,1,0:T(8,128)(2,1)}), bf16[16,32,128]{2,1,0:T(8,128)(2,1)S(1)}, u32[]{:S(2)}, u32[]{:S(2)}) %all-to-all-start.2) | async-done | bytes 131104 | tf_op jit(solution)/shard_map/all_to_all | solution.py:22
  82.2 3.5 %all-to-all-start.3 = ((bf16[4,32,2048]{2,1,0:T(8,128)(2,1)}), bf16[4,32,2048]{2,1,0:T(8,128)(2,1)S(1)}, u32[]{:S(2)}, u32[]{:S(2)}) async-start(bf16[4,32,2048]{2,1,0:T(8,128)(2,1)} %broadcast_in_dim.35), calls=%async_computation.3 | async-start | bytes 1048576 | tf_op jit(solution)/shard_map/all_to_all | solution.py:22
  85.8 1.9 %collective-permute-start.8 = (f32[2,128]{1,0:T(2,128)S(1)}, f32[2,128]{1,0:T(2,128)S(1)}, u32[]{:S(2)}, u32[]{:S(2)}) collective-permute-start(f32[2,128]{1,0:T(2,128)S(1)} %bitcast.83), channel_id=1, source_target_pairs={{0,4},{4,0},{1,5},{5,1},{2,6},{6,2},{3,7},{7,3},{8,12},{12,8},{9,1... | collective-permute-start | bytes 3080 | tf_op jit(solution)/shard_map/ppermute | solution.py:30
  87.7 6.0 %all-to-all-done.3 = bf16[4,32,2048]{2,1,0:T(8,128)(2,1)S(1)} async-done(((bf16[4,32,2048]{2,1,0:T(8,128)(2,1)}), bf16[4,32,2048]{2,1,0:T(8,128)(2,1)S(1)}, u32[]{:S(2)}, u32[]{:S(2)}) %all-to-all-start.3) | async-done | bytes 524320 | tf_op jit(solution)/shard_map/all_to_all | solution.py:22
  96.9 13.5 %all-to-all-start.4 = ((f32[64,2,128]{2,1,0:T(2,128)}), f32[64,2,128]{2,1,0:T(2,128)S(1)}, u32[]{:S(2)}, u32[]{:S(2)}) async-start(f32[64,2,128]{2,1,0:T(2,128)} %broadcast_in_dim.37), calls=%async_computation.4 | async-start | bytes 131072 | tf_op jit(solution)/shard_map/all_to_all | solution.py:22
  110.5 1.7 %fusion.1 = bf16[128,2048]{1,0:T(8,128)(2,1)S(1)} fusion(f32[128,2048]{1,0:T(8,128)} %fusion.47, bf16[2048,256]{1,0:T(8,128)(2,1)S(1)} %collective-permute-done.4, f32[128,256]{1,0:T(8,128)S(1)} %get-tuple-element.67, f32[128]{0:T(128)S(1)} %log_add_fusion.1, s32[256]{0:T(256)S(1)} %iota_add_fusion, s32[128]{0:T(128)S(1)} %select_reduce_fusion), kind=kOutput, calls=%fused_computation.3 | convolution fusion | flops 134873088 | bytes 2754560 | tf_op jit(solution)/shard_map/dot_general | solution.py:34
  112.3 5.1 %collective-permute-start.10 = (bf16[32,2048]{1,0:T(8,128)(2,1)S(1)}, bf16[32,2048]{1,0:T(8,128)(2,1)S(1)}, u32[]{:S(2)}, u32[]{:S(2)}) collective-permute-start(bf16[32,2048]{1,0:T(8,128)(2,1)S(1)} %get-tuple-element.41), channel_id=1, source_target_pairs={{0,16},{8,24},{16,0},{24,8},{1,17},{9,25},{17,1},{25,9},{2,18},{10... | collective-permute-start | bytes 393224 | tf_op jit(solution)/shard_map/ppermute | solution.py:30
  117.4 3.1 %collective-permute-start.11 = (bf16[32,2048]{1,0:T(8,128)(2,1)S(1)}, bf16[32,2048]{1,0:T(8,128)(2,1)S(1)}, u32[]{:S(2)}, u32[]{:S(2)}) collective-permute-start(bf16[32,2048]{1,0:T(8,128)(2,1)S(1)} %get-tuple-element.40), channel_id=1, source_target_pairs={{0,24},{8,16},{16,8},{24,0},{1,25},{9,17},{17,9},{25,1},{2,26},{10... | collective-permute-start | bytes 393224 | tf_op jit(solution)/shard_map/ppermute | solution.py:30
  120.5 1.9 %collective-permute-start.9 = (bf16[32,2048]{1,0:T(8,128)(2,1)S(1)}, bf16[32,2048]{1,0:T(8,128)(2,1)}, u32[]{:S(2)}, u32[]{:S(2)}) collective-permute-start(bf16[32,2048]{1,0:T(8,128)(2,1)S(1)} %get-tuple-element.39), channel_id=1, source_target_pairs={{0,8},{8,0},{16,24},{24,16},{1,9},{9,1},{17,25},{25,17},{2,10},{10... | collective-permute-start | bytes 393224 | tf_op jit(solution)/shard_map/ppermute | solution.py:30
  122.5 3.2 %all-to-all-done.4 = f32[64,2,128]{2,1,0:T(2,128)S(1)} async-done(((f32[64,2,128]{2,1,0:T(2,128)}), f32[64,2,128]{2,1,0:T(2,128)S(1)}, u32[]{:S(2)}, u32[]{:S(2)}) %all-to-all-start.4) | async-done | bytes 65568 | tf_op jit(solution)/shard_map/all_to_all | solution.py:22
  128.7 2.7 %collective-permute-start.12 = (bf16[128,1024]{1,0:T(8,128)(2,1)S(1)}, bf16[128,1024]{1,0:T(8,128)(2,1)S(1)}, u32[]{:S(2)}, u32[]{:S(2)}) collective-permute-start(bf16[128,1024]{1,0:T(8,128)(2,1)S(1)} %get-tuple-element.51), channel_id=1, source_target_pairs={{0,1},{1,0},{2,3},{3,2},{4,5},{5,4},{6,7},{7,6},{8,9},{9,8},{10,11... | collective-permute-start | bytes 786440 | tf_op jit(solution)/shard_map/ppermute | solution.py:30
  131.3 2.9 %collective-permute-start.13 = (bf16[128,1024]{1,0:T(8,128)(2,1)S(1)}, bf16[128,1024]{1,0:T(8,128)(2,1)S(1)}, u32[]{:S(2)}, u32[]{:S(2)}) collective-permute-start(bf16[128,1024]{1,0:T(8,128)(2,1)S(1)} %get-tuple-element.52), channel_id=1, source_target_pairs={{0,2},{1,3},{2,0},{3,1},{4,6},{5,7},{6,4},{7,5},{8,10},{9,11},{10,... | collective-permute-start | bytes 786440 | tf_op jit(solution)/shard_map/ppermute | solution.py:30
  134.2 4.9 %collective-permute-start.14 = (bf16[128,1024]{1,0:T(8,128)(2,1)S(1)}, bf16[128,1024]{1,0:T(8,128)(2,1)S(1)}, u32[]{:S(2)}, u32[]{:S(2)}) collective-permute-start(bf16[128,1024]{1,0:T(8,128)(2,1)S(1)} %get-tuple-element.53), channel_id=1, source_target_pairs={{0,3},{1,2},{2,1},{3,0},{4,7},{5,6},{6,5},{7,4},{8,11},{9,10},{10,... | collective-permute-start | bytes 786440 | tf_op jit(solution)/shard_map/ppermute | solution.py:30
  139.9 11.7 %all-to-all-start.5 = ((bf16[16,2,2048]{2,1,0:T(2,128)(2,1)}), bf16[16,2,2048]{2,1,0:T(2,128)(2,1)S(1)}, u32[]{:S(2)}, u32[]{:S(2)}) async-start(bf16[16,2,2048]{2,1,0:T(2,128)(2,1)} %reshape.264), calls=%async_computation.5 | async-start | bytes 262144 | tf_op jit(solution)/shard_map/all_to_all | solution.py:22
  153.5 1.9 %collective-permute-start.15 = (f32[512,256]{1,0:T(8,128)}, f32[512,256]{1,0:T(8,128)}, u32[]{:S(2)}, u32[]{:S(2)}) collective-permute-start(f32[512,256]{1,0:T(8,128)} %fusion.3), channel_id=1, source_target_pairs={{0,4},{4,0},{1,5},{5,1},{2,6},{6,2},{3,7},{7,3},{8,12},{12,8},{9,1... | collective-permute-start | bytes 1572872 | tf_op jit(solution)/shard_map/ppermute | solution.py:30
  155.4 9.4 %all-to-all-done.5 = bf16[16,2,2048]{2,1,0:T(2,128)(2,1)S(1)} async-done(((bf16[16,2,2048]{2,1,0:T(2,128)(2,1)}), bf16[16,2,2048]{2,1,0:T(2,128)(2,1)S(1)}, u32[]{:S(2)}, u32[]{:S(2)}) %all-to-all-start.5) | async-done | bytes 131104 | tf_op jit(solution)/shard_map/all_to_all | solution.py:22
  165.7 2.2 %convolution_add_fusion.2 = f32[512,256]{1,0:T(8,128)} fusion(f32[512,256]{1,0:T(8,128)} %collective-permute-done.15, bf16[512,1024]{1,0:T(8,128)(2,1)S(1)} %pad_maximum_fusion, bf16[128,1024]{1,0:T(8,128)(2,1)S(1)} %collective-permute-done.14, bf16[128,1024]{1,0:T(8,128)(2,1)S(1)} %collective-permute-done.13, ...), kind=kOutput, calls=%fused_computation.4 | convolution fusion | flops 135921664 | bytes 2621440 | tf_op jit(solution)/shard_map/dot_general | solution.py:34
  (105 shorter events, 21.7 us)
Async XLA Ops:
  0.6 18.5 %copy-start.3 = (bf16[5632,16]{0,1:T(8,128)(2,1)S(1)}, bf16[5632,16]{0,1:T(8,128)(2,1)}, u32[]{:S(2)}) copy-start(bf16[5632,16]{0,1:T(8,128)(2,1)} %param.10) | copy-start | bytes 540676
  3.9 39.0 %all-to-all-start = ((bf16[16,48,256]{2,1,0:T(8,128)(2,1)}), bf16[16,48,256]{2,1,0:T(8,128)(2,1)S(1)}, u32[]{:S(2)}, u32[]{:S(2)}) async-start(bf16[16,48,256]{2,1,0:T(8,128)(2,1)} %pad_add_fusion), calls=%async_computation | async-start | bytes 786432 | tf_op jit(solution)/shard_map/all_to_all | solution.py:22
  21.3 3.2 %collective-permute-start = (bf16[1,4,16,768]{3,2,1,0:T(8,128)(2,1)S(1)}, bf16[1,4,16,768]{3,2,1,0:T(8,128)(2,1)S(1)}, u32[]{:S(2)}, u32[]{:S(2)}) collective-permute-start(bf16[1,4,16,768]{3,2,1,0:T(8,128)(2,1)S(1)} %dynamic-slice_bitcast_fusion), channel_id=1, source_target_pairs={{0,4},{4,0},{1,5},{5,1},{2,6},{6,2},{3,7},{7,3},{8,12},{12,8},{9,1... | collective-permute-start | bytes 294920 | tf_op jit(solution)/shard_map/ppermute | solution.py:30
  23.4 21.3 %copy-start.1 = (bf16[2048,256]{1,0:T(8,128)(2,1)S(1)}, bf16[2048,256]{1,0:T(8,128)(2,1)}, u32[]{:S(2)}) copy-start(bf16[2048,256]{1,0:T(8,128)(2,1)} %param.12) | copy-start | bytes 3145732
  23.4 23.2 %copy-start.11 = (s32[256]{0:T(256)S(1)}, s32[256]{0:T(256)}, u32[]{:S(2)}) copy-start(s32[256]{0:T(256)} %param.14) | copy-start | bytes 3076
  24.6 10.5 %collective-permute-start.1 = (bf16[1,2,16,768]{3,2,1,0:T(8,128)(2,1)S(1)}, bf16[1,2,16,768]{3,2,1,0:T(8,128)(2,1)S(1)}, u32[]{:S(2)}, u32[]{:S(2)}) collective-permute-start(bf16[1,2,16,768]{3,2,1,0:T(8,128)(2,1)S(1)} %get-tuple-element.49), channel_id=1, source_target_pairs={{0,8},{8,0},{16,24},{24,16},{1,9},{9,1},{17,25},{25,17},{2,10},{10... | collective-permute-start | bytes 147464 | tf_op jit(solution)/shard_map/ppermute | solution.py:30
  28.0 7.5 %collective-permute-start.2 = (bf16[1,2,16,768]{3,2,1,0:T(8,128)(2,1)S(1)}, bf16[1,2,16,768]{3,2,1,0:T(8,128)(2,1)S(1)}, u32[]{:S(2)}, u32[]{:S(2)}) collective-permute-start(bf16[1,2,16,768]{3,2,1,0:T(8,128)(2,1)S(1)} %get-tuple-element.50), channel_id=1, source_target_pairs={{0,16},{8,24},{16,0},{24,8},{1,17},{9,25},{17,1},{25,9},{2,18},{10... | collective-permute-start | bytes 147464 | tf_op jit(solution)/shard_map/ppermute | solution.py:30
  32.7 7.2 %collective-permute-start.3 = (bf16[1,2,16,768]{3,2,1,0:T(8,128)(2,1)S(1)}, bf16[1,2,16,768]{3,2,1,0:T(8,128)(2,1)S(1)}, u32[]{:S(2)}, u32[]{:S(2)}) collective-permute-start(bf16[1,2,16,768]{3,2,1,0:T(8,128)(2,1)S(1)} %get-tuple-element.48), channel_id=1, source_target_pairs={{0,24},{8,16},{16,8},{24,0},{1,25},{9,17},{17,9},{25,1},{2,26},{10... | collective-permute-start | bytes 147464 | tf_op jit(solution)/shard_map/ppermute | solution.py:30
  44.7 21.3 %collective-permute-start.4 = (bf16[2048,256]{1,0:T(8,128)(2,1)S(1)}, bf16[2048,256]{1,0:T(8,128)(2,1)S(1)}, u32[]{:S(2)}, u32[]{:S(2)}) collective-permute-start(bf16[2048,256]{1,0:T(8,128)(2,1)S(1)} %copy-done.1), channel_id=1, source_target_pairs={{0,4},{4,0},{1,5},{5,1},{2,6},{6,2},{3,7},{7,3},{8,12},{12,8},{9,1... | collective-permute-start | bytes 3145736 | tf_op jit(solution)/shard_map/ppermute | solution.py:30
  46.9 10.5 %all-to-all-start.1 = ((f32[8,32,128]{2,1,0:T(8,128)}), f32[8,32,128]{2,1,0:T(8,128)S(1)}, u32[]{:S(2)}, u32[]{:S(2)}) async-start(f32[8,32,128]{2,1,0:T(8,128)} %bitcast.14), calls=%async_computation.1 | async-start | bytes 262144 | tf_op jit(solution)/shard_map/all_to_all | solution.py:22
  58.1 22.3 %all-to-all-start.2 = ((bf16[16,32,128]{2,1,0:T(8,128)(2,1)}), bf16[16,32,128]{2,1,0:T(8,128)(2,1)S(1)}, u32[]{:S(2)}, u32[]{:S(2)}) async-start(bf16[16,32,128]{2,1,0:T(8,128)(2,1)} %broadcast_in_dim.32), calls=%async_computation.2 | async-start | bytes 262144 | tf_op jit(solution)/shard_map/all_to_all | solution.py:22
  66.5 14.8 %copy-start.10 = (f32[2048]{0:T(1024)S(1)}, f32[2048]{0:T(1024)}, u32[]{:S(2)}) copy-start(f32[2048]{0:T(1024)} %param.11) | copy-start | bytes 24580
  66.6 13.9 %collective-permute-start.5 = (bf16[32,2048]{1,0:T(8,128)(2,1)S(1)}, bf16[32,2048]{1,0:T(8,128)(2,1)S(1)}, u32[]{:S(2)}, u32[]{:S(2)}) collective-permute-start(bf16[32,2048]{1,0:T(8,128)(2,1)S(1)} %get-tuple-element.44), channel_id=1, source_target_pairs={{0,8},{8,0},{16,24},{24,16},{1,9},{9,1},{17,25},{25,17},{2,10},{10... | collective-permute-start | bytes 393224 | tf_op jit(solution)/shard_map/ppermute | solution.py:30
  69.0 11.4 %collective-permute-start.6 = (bf16[32,2048]{1,0:T(8,128)(2,1)S(1)}, bf16[32,2048]{1,0:T(8,128)(2,1)S(1)}, u32[]{:S(2)}, u32[]{:S(2)}) collective-permute-start(bf16[32,2048]{1,0:T(8,128)(2,1)S(1)} %get-tuple-element.43), channel_id=1, source_target_pairs={{0,16},{8,24},{16,0},{24,8},{1,17},{9,25},{17,1},{25,9},{2,18},{10... | collective-permute-start | bytes 393224 | tf_op jit(solution)/shard_map/ppermute | solution.py:30
  73.0 8.1 %collective-permute-start.7 = (bf16[32,2048]{1,0:T(8,128)(2,1)S(1)}, bf16[32,2048]{1,0:T(8,128)(2,1)S(1)}, u32[]{:S(2)}, u32[]{:S(2)}) collective-permute-start(bf16[32,2048]{1,0:T(8,128)(2,1)S(1)} %get-tuple-element.42), channel_id=1, source_target_pairs={{0,24},{8,16},{16,8},{24,0},{1,25},{9,17},{17,9},{25,1},{2,26},{10... | collective-permute-start | bytes 393224 | tf_op jit(solution)/shard_map/ppermute | solution.py:30
  80.5 1.7 %copy-start.6 = (bf16[32,2048]{1,0:T(8,128)(2,1)}, bf16[32,2048]{1,0:T(8,128)(2,1)S(1)}, u32[]{:S(2)}) copy-start(bf16[32,2048]{1,0:T(8,128)(2,1)S(1)} %collective-permute-done.6) | copy-start | bytes 393220
  81.1 1.1 copy-start.8
  81.2 4.5 %copy-start.12 = (f32[256]{0:T(256)S(1)}, f32[256]{0:T(256)}, u32[]{:S(2)}) copy-start(f32[256]{0:T(256)} %param.13) | copy-start | bytes 3076
  82.2 11.5 %all-to-all-start.3 = ((bf16[4,32,2048]{2,1,0:T(8,128)(2,1)}), bf16[4,32,2048]{2,1,0:T(8,128)(2,1)S(1)}, u32[]{:S(2)}, u32[]{:S(2)}) async-start(bf16[4,32,2048]{2,1,0:T(8,128)(2,1)} %broadcast_in_dim.35), calls=%async_computation.3 | async-start | bytes 1048576 | tf_op jit(solution)/shard_map/all_to_all | solution.py:22
  85.8 8.4 %collective-permute-start.8 = (f32[2,128]{1,0:T(2,128)S(1)}, f32[2,128]{1,0:T(2,128)S(1)}, u32[]{:S(2)}, u32[]{:S(2)}) collective-permute-start(f32[2,128]{1,0:T(2,128)S(1)} %bitcast.83), channel_id=1, source_target_pairs={{0,4},{4,0},{1,5},{5,1},{2,6},{6,2},{3,7},{7,3},{8,12},{12,8},{9,1... | collective-permute-start | bytes 3080 | tf_op jit(solution)/shard_map/ppermute | solution.py:30
  96.9 28.7 %all-to-all-start.4 = ((f32[64,2,128]{2,1,0:T(2,128)}), f32[64,2,128]{2,1,0:T(2,128)S(1)}, u32[]{:S(2)}, u32[]{:S(2)}) async-start(f32[64,2,128]{2,1,0:T(2,128)} %broadcast_in_dim.37), calls=%async_computation.4 | async-start | bytes 131072 | tf_op jit(solution)/shard_map/all_to_all | solution.py:22
  112.2 15.2 %copy-start.5 = (bf16[32,2048]{1,0:T(8,128)(2,1)S(1)}, bf16[32,2048]{1,0:T(8,128)(2,1)}, u32[]{:S(2)}) copy-start(bf16[32,2048]{1,0:T(8,128)(2,1)} %copy-done.4) | copy-start | bytes 393220
  112.2 15.2 %copy-start.7 = (bf16[32,2048]{1,0:T(8,128)(2,1)S(1)}, bf16[32,2048]{1,0:T(8,128)(2,1)}, u32[]{:S(2)}) copy-start(bf16[32,2048]{1,0:T(8,128)(2,1)} %copy-done.6) | copy-start | bytes 393220
  112.3 15.2 %copy-start.9 = (bf16[32,2048]{1,0:T(8,128)(2,1)S(1)}, bf16[32,2048]{1,0:T(8,128)(2,1)}, u32[]{:S(2)}) copy-start(bf16[32,2048]{1,0:T(8,128)(2,1)} %copy-done.8) | copy-start | bytes 393220
  112.3 13.8 %collective-permute-start.10 = (bf16[32,2048]{1,0:T(8,128)(2,1)S(1)}, bf16[32,2048]{1,0:T(8,128)(2,1)S(1)}, u32[]{:S(2)}, u32[]{:S(2)}) collective-permute-start(bf16[32,2048]{1,0:T(8,128)(2,1)S(1)} %get-tuple-element.41), channel_id=1, source_target_pairs={{0,16},{8,24},{16,0},{24,8},{1,17},{9,25},{17,1},{25,9},{2,18},{10... | collective-permute-start | bytes 393224 | tf_op jit(solution)/shard_map/ppermute | solution.py:30
  117.4 8.7 %collective-permute-start.11 = (bf16[32,2048]{1,0:T(8,128)(2,1)S(1)}, bf16[32,2048]{1,0:T(8,128)(2,1)S(1)}, u32[]{:S(2)}, u32[]{:S(2)}) collective-permute-start(bf16[32,2048]{1,0:T(8,128)(2,1)S(1)} %get-tuple-element.40), channel_id=1, source_target_pairs={{0,24},{8,16},{16,8},{24,0},{1,25},{9,17},{17,9},{25,1},{2,26},{10... | collective-permute-start | bytes 393224 | tf_op jit(solution)/shard_map/ppermute | solution.py:30
  120.5 7.0 %collective-permute-start.9 = (bf16[32,2048]{1,0:T(8,128)(2,1)S(1)}, bf16[32,2048]{1,0:T(8,128)(2,1)}, u32[]{:S(2)}, u32[]{:S(2)}) collective-permute-start(bf16[32,2048]{1,0:T(8,128)(2,1)S(1)} %get-tuple-element.39), channel_id=1, source_target_pairs={{0,8},{8,0},{16,24},{24,16},{1,9},{9,1},{17,25},{25,17},{2,10},{10... | collective-permute-start | bytes 393224 | tf_op jit(solution)/shard_map/ppermute | solution.py:30
  128.7 23.6 %collective-permute-start.12 = (bf16[128,1024]{1,0:T(8,128)(2,1)S(1)}, bf16[128,1024]{1,0:T(8,128)(2,1)S(1)}, u32[]{:S(2)}, u32[]{:S(2)}) collective-permute-start(bf16[128,1024]{1,0:T(8,128)(2,1)S(1)} %get-tuple-element.51), channel_id=1, source_target_pairs={{0,1},{1,0},{2,3},{3,2},{4,5},{5,4},{6,7},{7,6},{8,9},{9,8},{10,11... | collective-permute-start | bytes 786440 | tf_op jit(solution)/shard_map/ppermute | solution.py:30
  131.3 20.9 %collective-permute-start.13 = (bf16[128,1024]{1,0:T(8,128)(2,1)S(1)}, bf16[128,1024]{1,0:T(8,128)(2,1)S(1)}, u32[]{:S(2)}, u32[]{:S(2)}) collective-permute-start(bf16[128,1024]{1,0:T(8,128)(2,1)S(1)} %get-tuple-element.52), channel_id=1, source_target_pairs={{0,2},{1,3},{2,0},{3,1},{4,6},{5,7},{6,4},{7,5},{8,10},{9,11},{10,... | collective-permute-start | bytes 786440 | tf_op jit(solution)/shard_map/ppermute | solution.py:30
  134.2 18.0 %collective-permute-start.14 = (bf16[128,1024]{1,0:T(8,128)(2,1)S(1)}, bf16[128,1024]{1,0:T(8,128)(2,1)S(1)}, u32[]{:S(2)}, u32[]{:S(2)}) collective-permute-start(bf16[128,1024]{1,0:T(8,128)(2,1)S(1)} %get-tuple-element.53), channel_id=1, source_target_pairs={{0,3},{1,2},{2,1},{3,0},{4,7},{5,6},{6,5},{7,4},{8,11},{9,10},{10,... | collective-permute-start | bytes 786440 | tf_op jit(solution)/shard_map/ppermute | solution.py:30
  139.9 24.9 %all-to-all-start.5 = ((bf16[16,2,2048]{2,1,0:T(2,128)(2,1)}), bf16[16,2,2048]{2,1,0:T(2,128)(2,1)S(1)}, u32[]{:S(2)}, u32[]{:S(2)}) async-start(bf16[16,2,2048]{2,1,0:T(2,128)(2,1)} %reshape.264), calls=%async_computation.5 | async-start | bytes 262144 | tf_op jit(solution)/shard_map/all_to_all | solution.py:22
  153.5 12.2 %collective-permute-start.15 = (f32[512,256]{1,0:T(8,128)}, f32[512,256]{1,0:T(8,128)}, u32[]{:S(2)}, u32[]{:S(2)}) collective-permute-start(f32[512,256]{1,0:T(8,128)} %fusion.3), channel_id=1, source_target_pairs={{0,4},{4,0},{1,5},{5,1},{2,6},{6,2},{3,7},{7,3},{8,12},{12,8},{9,1... | collective-permute-start | bytes 1572872 | tf_op jit(solution)/shard_map/ppermute | solution.py:30
  (3 other events, 2.2 us)
where the time goes:
time: 169 us; the launch traced here: 168 us
  starting transfers between devices  105 us (62%)
  waiting for transfers between devices  37.8 us (22%)
  matrix products  10.2 us (6%)
  local copies, waits for them, and re-layouts  8.24 us (5%)
  other arithmetic  5.06 us (3%)
    all_to_all x6, starting transfers between devices, exchange(): return lax.all_to_all(blocks, axes, split_axis=0, concat_axis=0, tiled=True)  56.1 us
    ppermute x16, starting transfers between devices, partner(): lax.ppermute(array, axes, [(k, k ^ step) for k in range(lax.axis_size(axe...  49 us
    all_to_all x6, waiting for transfers between devices, exchange(): return lax.all_to_all(blocks, axes, split_axis=0, concat_axis=0, tiled=True)  30 us
    dot_general x10, matrix products, dot(): lax.dot_general(a, b, (((da,), (db,)), ((), ())), preferred_element_type=...  10.2 us
    ppermute x16, waiting for transfers between devices, partner(): lax.ppermute(array, axes, [(k, k ^ step) for k in range(lax.axis_size(axe...  7.84 us
  transfers between devices with their start and end apart: 22, of which 11 were waited for; matrix products, arithmetic and copies ran while one was open for 7% of the time, Pallas kernels for 0%

commit v1 on v0

--- a/solution.py
+++ b/solution.py
@@ -8,7 +8,6 @@
 
 Z, X, C = "vp_0", "vp_1", "vp_2"
 Q = ("vp_1", "vp_2")
-ZX = ("vp_0", "vp_1")
 VP = ("vp_0", "vp_1", "vp_2")
 DP_VP = ("dp", "vp_0", "vp_1", "vp_2")
 
@@ -32,6 +31,12 @@
 
 def dot(a, b, da, db):
     return lax.dot_general(a, b, (((da,), (db,)), ((), ())), preferred_element_type=f32)
+
+
+def merged(stats):
+    top = jnp.max(stats[:, 0], axis=0)
+    lse = top + jnp.log(jnp.sum(jnp.exp(stats[:, 0] - top), axis=0))
+    return jnp.stack([lse, jnp.sum(stats[:, 1], axis=0)])
 
 
 def blocks_over_x(rows, x, span):
@@ -105,21 +110,24 @@
     normed = (values * inv * final_gain).astype(bf16)
     normed = shared(normed, X, nx).reshape(half, width)
 
+    feat_group, far = width // ny, ny // 2
+    slices = [lax.dynamic_slice_in_dim(normed, (y ^ k) * feat_group, feat_group, 1) for k in range(ny)]
+    slices[far] = partner(slices[far], "dp", far)
+
     scores = [dot(normed, v, 1, 0) + b for v, b in zip(vocab, bias)]
     top = jnp.maximum(jnp.max(scores[0], axis=1), jnp.max(scores[1], axis=1))
     total = sum(jnp.sum(jnp.exp(s - top[:, None]), axis=1) for s in scores)
     goal = sum(jnp.sum(jnp.where(h, s, 0.0), axis=1) for h, s in zip(hit, scores))
     local = top + jnp.log(total)
-    stats = shared(jnp.stack([local, goal]), ZX, nz * nx)
+    near = shared(jnp.stack([local, goal]), X, nx)
     terms = sum(
         dot(jnp.where(h, 0.0, jnp.exp(s - local[:, None])).astype(bf16), v, 1, 1)
         for h, s, v in zip(hit, scores, vocab)
     ).astype(bf16)
     terms = blocks_over_x(terms, x, span)
 
-    top = jnp.max(stats[:, 0], axis=0)
-    lse = top + jnp.log(jnp.sum(jnp.exp(stats[:, 0] - top), axis=0))
-    goal = jnp.sum(stats[:, 1], axis=0)
+    stats = shared(merged(near), Z, nz)
+    lse, goal = merged(stats)
     losses = lse - goal + zloss_weight * lse * lse
     losses = lax.dynamic_slice_in_dim(losses, x * span + z * own, own)
     scale = 1.0 + 2.0 * zloss_weight * lse
@@ -127,25 +135,26 @@
         (jnp.exp(s - lse[:, None]) * scale[:, None] - jnp.where(h, 1.0, 0.0)).astype(bf16)
         for s, h in zip(scores, hit)
     ]
-    shares = jnp.concatenate([jnp.exp(stats[:, 0] - lse) * scale, (jnp.exp(goal - lse) * scale - 1.0)[None]])
+    shares = jnp.concatenate([jnp.exp(near[:, 0] - lse) * scale, (jnp.exp(goal - lse) * scale - 1.0)[None]])
     shares = lax.dynamic_slice_in_dim(shares, x * span, span, 1)
     row_x = shares[-1][:, None] * goal_rows
     for step in range(nx):
-        share = lax.dynamic_slice_in_dim(shares, z * nx + (x ^ step), 1)
+        share = lax.dynamic_slice_in_dim(shares, x ^ step, 1)
         row_x = row_x + share.reshape(span, 1) * terms[step].astype(f32)
     row_x = row_x.astype(bf16)
 
     row_x, *dscore = lax.optimization_barrier((row_x, *dscore))
-    feat_group = width // ny
-    pieces = []
+    theirs, ours = 0.0, 0.0
     for step in range(ny):
-        piece = lax.dynamic_slice_in_dim(normed, (y ^ step) * feat_group, feat_group, 1)
-        piece = jnp.concatenate([piece, *dscore], axis=1)
-        pieces.append(partner(piece, "dp", step) if step else piece)
-    pieces = jnp.concatenate(pieces)
-    at = feat_group + ncols
-    theirs = dot(pieces[:, :feat_group], pieces[:, at:], 0, 0)
-    grad_vocab = dot(pieces[:, :feat_group], pieces[:, feat_group:at], 0, 0) + partner(theirs, C, 1)
+        piece, cols_of = slices[step], jnp.concatenate(dscore, axis=1)
+        if step == far:
+            cols_of = partner(cols_of, "dp", step)
+        elif step:
+            piece = partner(jnp.concatenate([piece, cols_of], axis=1), "dp", step)
+            piece, cols_of = piece[:, :feat_group], piece[:, feat_group:]
+        theirs = theirs + dot(piece, cols_of[:, ncols:], 0, 0)
+        ours = ours + dot(piece, cols_of[:, :ncols], 0, 0)
+    grad_vocab = lax.optimization_barrier(ours) + partner(theirs, C, 1)
 
     row_z = exchange(row_x.reshape(nz, own, width), Z)
     dnormed = jnp.sum(row_z.astype(f32), axis=0)

time: 169 us -> 176 us (1.041)
  the two profiles are of different devices: /device:TPU:24 before, /device:TPU:2 now
where the time goes in v1:
time: 176 us; the launch traced here: 174 us
  starting transfers between devices  106 us (60%)
  waiting for transfers between devices  39.6 us (22%)
  local copies, waits for them, and re-layouts  11.6 us (7%)
  matrix products  8.91 us (5%)
  other arithmetic  6.49 us (4%)
    all_to_all x7, starting transfers between devices, exchange(): return lax.all_to_all(blocks, axes, split_axis=0, concat_axis=0, tiled=True)  54.4 us
    ppermute x17, starting transfers between devices, partner(): lax.ppermute(array, axes, [(k, k ^ step) for k in range(lax.axis_size(axe...  51.8 us
    all_to_all x7, waiting for transfers between devices, exchange(): return lax.all_to_all(blocks, axes, split_axis=0, concat_axis=0, tiled=True)  34.7 us
    dot_general x16, matrix products, dot(): lax.dot_general(a, b, (((da,), (db,)), ((), ())), preferred_element_type=...  8.91 us
    ppermute x17, waiting for transfers between devices, partner(): lax.ppermute(array, axes, [(k, k ^ step) for k in range(lax.axis_size(axe...  4.94 us
    unnamed x28, local copies, waits for them, and re-layouts  4.13 us
  transfers between devices with their start and end apart: 24, of which 11 were waited for; matrix products, arithmetic and copies ran while one was open for 9% of the time, Pallas kernels for 0%

profile of v1, /device:TPU:2, one launch (start us, length us, event | category | flops | bytes accessed | tf_op | source)
XLA Modules:
  0.0 174.2 jit_solution(3877214326471216636)
XLA Ops:
  3.9 15.3 %all-to-all-start = ((bf16[16,48,256]{2,1,0:T(8,128)(2,1)}), bf16[16,48,256]{2,1,0:T(8,128)(2,1)S(1)}, u32[]{:S(2)}, u32[]{:S(2)}) async-start(bf16[16,48,256]{2,1,0:T(8,128)(2,1)} %pad_add_fusion), calls=%async_computation | async-start | bytes 786432 | tf_op jit(solution)/shard_map/all_to_all | solution.py:21
  21.5 1.9 %collective-permute-start = (bf16[1,4,16,768]{3,2,1,0:T(8,128)(2,1)S(1)}, bf16[1,4,16,768]{3,2,1,0:T(8,128)(2,1)S(1)}, u32[]{:S(2)}, u32[]{:S(2)}) collective-permute-start(bf16[1,4,16,768]{3,2,1,0:T(8,128)(2,1)S(1)} %dynamic-slice_bitcast_fusion), channel_id=1, source_target_pairs={{0,4},{4,0},{1,5},{5,1},{2,6},{6,2},{3,7},{7,3},{8,12},{12,8},{9,1... | collective-permute-start | bytes 294920 | tf_op jit(solution)/shard_map/ppermute | solution.py:29
  24.7 2.4 %collective-permute-start.1 = (bf16[1,2,16,768]{3,2,1,0:T(8,128)(2,1)S(1)}, bf16[1,2,16,768]{3,2,1,0:T(8,128)(2,1)S(1)}, u32[]{:S(2)}, u32[]{:S(2)}) collective-permute-start(bf16[1,2,16,768]{3,2,1,0:T(8,128)(2,1)S(1)} %get-tuple-element.48), channel_id=1, source_target_pairs={{0,8},{8,0},{16,24},{24,16},{1,9},{9,1},{17,25},{25,17},{2,10},{10... | collective-permute-start | bytes 147464 | tf_op jit(solution)/shard_map/ppermute | solution.py:29
  27.2 4.3 %collective-permute-start.2 = (bf16[1,2,16,768]{3,2,1,0:T(8,128)(2,1)S(1)}, bf16[1,2,16,768]{3,2,1,0:T(8,128)(2,1)S(1)}, u32[]{:S(2)}, u32[]{:S(2)}) collective-permute-start(bf16[1,2,16,768]{3,2,1,0:T(8,128)(2,1)S(1)} %get-tuple-element.49), channel_id=1, source_target_pairs={{0,16},{8,24},{16,0},{24,8},{1,17},{9,25},{17,1},{25,9},{2,18},{10... | collective-permute-start | bytes 147464 | tf_op jit(solution)/shard_map/ppermute | solution.py:29
  31.5 2.4 %collective-permute-start.3 = (bf16[1,2,16,768]{3,2,1,0:T(8,128)(2,1)S(1)}, bf16[1,2,16,768]{3,2,1,0:T(8,128)(2,1)S(1)}, u32[]{:S(2)}, u32[]{:S(2)}) collective-permute-start(bf16[1,2,16,768]{3,2,1,0:T(8,128)(2,1)S(1)} %get-tuple-element.47), channel_id=1, source_target_pairs={{0,24},{8,16},{16,8},{24,0},{1,25},{9,17},{17,9},{25,1},{2,26},{10... | collective-permute-start | bytes 147464 | tf_op jit(solution)/shard_map/ppermute | solution.py:29
  34.7 2.8 %collective-permute-done.3 = bf16[1,2,16,768]{3,2,1,0:T(8,128)(2,1)S(1)} collective-permute-done((bf16[1,2,16,768]{3,2,1,0:T(8,128)(2,1)S(1)}, bf16[1,2,16,768]{3,2,1,0:T(8,128)(2,1)S(1)}, u32[]{:S(2)}, u32[]{:S(2)}) %collective-permute-start.3) | collective-permute-done | bytes 49184 | tf_op jit(solution)/shard_map/ppermute | solution.py:29
  37.5 5.6 %all-to-all-done = bf16[16,48,256]{2,1,0:T(8,128)(2,1)S(1)} async-done(((bf16[16,48,256]{2,1,0:T(8,128)(2,1)}), bf16[16,48,256]{2,1,0:T(8,128)(2,1)S(1)}, u32[]{:S(2)}, u32[]{:S(2)}) %all-to-all-start) | async-done | bytes 393248 | tf_op jit(solution)/shard_map/all_to_all | solution.py:21
  44.8 1.9 %collective-permute-start.4 = (bf16[2048,256]{1,0:T(8,128)(2,1)S(1)}, bf16[2048,256]{1,0:T(8,128)(2,1)S(1)}, u32[]{:S(2)}, u32[]{:S(2)}) collective-permute-start(bf16[2048,256]{1,0:T(8,128)(2,1)S(1)} %copy-done.1), channel_id=1, source_target_pairs={{0,4},{4,0},{1,5},{5,1},{2,6},{6,2},{3,7},{7,3},{8,12},{12,8},{9,1... | collective-permute-start | bytes 3145736 | tf_op jit(solution)/shard_map/ppermute | solution.py:29
  47.7 4.9 %all-to-all-start.1 = ((f32[8,32,128]{2,1,0:T(8,128)}), f32[8,32,128]{2,1,0:T(8,128)S(1)}, u32[]{:S(2)}, u32[]{:S(2)}) async-start(f32[8,32,128]{2,1,0:T(8,128)} %bitcast.14), calls=%async_computation.1 | async-start | bytes 262144 | tf_op jit(solution)/shard_map/all_to_all | solution.py:21
  53.9 3.4 %all-to-all-done.1 = f32[8,32,128]{2,1,0:T(8,128)S(1)} async-done(((f32[8,32,128]{2,1,0:T(8,128)}), f32[8,32,128]{2,1,0:T(8,128)S(1)}, u32[]{:S(2)}, u32[]{:S(2)}) %all-to-all-start.1) | async-done | bytes 131104 | tf_op jit(solution)/shard_map/all_to_all | solution.py:21
  58.0 7.8 %all-to-all-start.2 = ((bf16[16,32,128]{2,1,0:T(8,128)(2,1)}), bf16[16,32,128]{2,1,0:T(8,128)(2,1)S(1)}, u32[]{:S(2)}, u32[]{:S(2)}) async-start(bf16[16,32,128]{2,1,0:T(8,128)(2,1)} %broadcast_in_dim.35), calls=%async_computation.2 | async-start | bytes 262144 | tf_op jit(solution)/shard_map/all_to_all | solution.py:21
  66.4 3.4 %collective-permute-start.5 = (bf16[32,2048]{1,0:T(8,128)(2,1)S(1)}, bf16[32,2048]{1,0:T(8,128)(2,1)S(1)}, u32[]{:S(2)}, u32[]{:S(2)}) collective-permute-start(bf16[32,2048]{1,0:T(8,128)(2,1)S(1)} %get-tuple-element.43), channel_id=1, source_target_pairs={{0,8},{8,0},{16,24},{24,16},{1,9},{9,1},{17,25},{25,17},{2,10},{10... | collective-permute-start | bytes 393224 | tf_op jit(solution)/shard_map/ppermute | solution.py:29
  69.8 2.1 %collective-permute-start.6 = (bf16[32,2048]{1,0:T(8,128)(2,1)S(1)}, bf16[32,2048]{1,0:T(8,128)(2,1)S(1)}, u32[]{:S(2)}, u32[]{:S(2)}) collective-permute-start(bf16[32,2048]{1,0:T(8,128)(2,1)S(1)} %get-tuple-element.42), channel_id=1, source_target_pairs={{0,16},{8,24},{16,0},{24,8},{1,17},{9,25},{17,1},{25,9},{2,18},{10... | collective-permute-start | bytes 393224 | tf_op jit(solution)/shard_map/ppermute | solution.py:29
  71.9 3.7 %collective-permute-start.7 = (bf16[32,2048]{1,0:T(8,128)(2,1)S(1)}, bf16[32,2048]{1,0:T(8,128)(2,1)S(1)}, u32[]{:S(2)}, u32[]{:S(2)}) collective-permute-start(bf16[32,2048]{1,0:T(8,128)(2,1)S(1)} %get-tuple-element.41), channel_id=1, source_target_pairs={{0,24},{8,16},{16,8},{24,0},{1,25},{9,17},{17,9},{25,1},{2,26},{10... | collective-permute-start | bytes 393224 | tf_op jit(solution)/shard_map/ppermute | solution.py:29
  76.4 1.9 %collective-permute-start.8 = (f32[2,128]{1,0:T(2,128)S(1)}, f32[2,128]{1,0:T(2,128)S(1)}, u32[]{:S(2)}, u32[]{:S(2)}) collective-permute-start(f32[2,128]{1,0:T(2,128)S(1)} %bitcast.99), channel_id=1, source_target_pairs={{0,4},{4,0},{1,5},{5,1},{2,6},{6,2},{3,7},{7,3},{8,12},{12,8},{9,1... | collective-permute-start | bytes 3080 | tf_op jit(solution)/shard_map/ppermute | solution.py:29
  78.3 2.0 %all-to-all-done.2 = bf16[16,32,128]{2,1,0:T(8,128)(2,1)S(1)} async-done(((bf16[16,32,128]{2,1,0:T(8,128)(2,1)}), bf16[16,32,128]{2,1,0:T(8,128)(2,1)S(1)}, u32[]{:S(2)}, u32[]{:S(2)}) %all-to-all-start.2) | async-done | bytes 131104 | tf_op jit(solution)/shard_map/all_to_all | solution.py:21
  82.1 5.3 %all-to-all-start.3 = ((bf16[4,32,2048]{2,1,0:T(8,128)(2,1)}), bf16[4,32,2048]{2,1,0:T(8,128)(2,1)S(1)}, u32[]{:S(2)}, u32[]{:S(2)}) async-start(bf16[4,32,2048]{2,1,0:T(8,128)(2,1)} %broadcast_in_dim.37), calls=%async_computation.3 | async-start | bytes 1048576 | tf_op jit(solution)/shard_map/all_to_all | solution.py:21
  88.3 6.9 %all-to-all-done.3 = bf16[4,32,2048]{2,1,0:T(8,128)(2,1)S(1)} async-done(((bf16[4,32,2048]{2,1,0:T(8,128)(2,1)}), bf16[4,32,2048]{2,1,0:T(8,128)(2,1)S(1)}, u32[]{:S(2)}, u32[]{:S(2)}) %all-to-all-start.3) | async-done | bytes 524320 | tf_op jit(solution)/shard_map/all_to_all | solution.py:21
  98.3 4.7 %all-to-all-start.4 = ((f32[4,2,128]{2,1,0:T(2,128)}), f32[4,2,128]{2,1,0:T(2,128)S(1)}, u32[]{:S(2)}, u32[]{:S(2)}) async-start(f32[4,2,128]{2,1,0:T(2,128)} %broadcast_in_dim.39), calls=%async_computation.4 | async-start | bytes 8192 | tf_op jit(solution)/shard_map/all_to_all | solution.py:21
  103.0 1.7 fusion.1
  104.7 4.0 %collective-permute-start.10 = (bf16[32,2048]{1,0:T(8,128)(2,1)S(1)}, bf16[32,2048]{1,0:T(8,128)(2,1)S(1)}, u32[]{:S(2)}, u32[]{:S(2)}) collective-permute-start(bf16[32,2048]{1,0:T(8,128)(2,1)S(1)} %get-tuple-element.40), channel_id=1, source_target_pairs={{0,16},{8,24},{16,0},{24,8},{1,17},{9,25},{17,1},{25,9},{2,18},{10... | collective-permute-start | bytes 393224 | tf_op jit(solution)/shard_map/ppermute | solution.py:29
  108.7 1.9 %collective-permute-start.11 = (bf16[32,2048]{1,0:T(8,128)(2,1)S(1)}, bf16[32,2048]{1,0:T(8,128)(2,1)S(1)}, u32[]{:S(2)}, u32[]{:S(2)}) collective-permute-start(bf16[32,2048]{1,0:T(8,128)(2,1)S(1)} %get-tuple-element.39), channel_id=1, source_target_pairs={{0,24},{8,16},{16,8},{24,0},{1,25},{9,17},{17,9},{25,1},{2,26},{10... | collective-permute-start | bytes 393224 | tf_op jit(solution)/shard_map/ppermute | solution.py:29
  110.6 4.5 %collective-permute-start.9 = (bf16[32,2048]{1,0:T(8,128)(2,1)S(1)}, bf16[32,2048]{1,0:T(8,128)(2,1)S(1)}, u32[]{:S(2)}, u32[]{:S(2)}) collective-permute-start(bf16[32,2048]{1,0:T(8,128)(2,1)S(1)} %get-tuple-element.38), channel_id=1, source_target_pairs={{0,8},{8,0},{16,24},{24,16},{1,9},{9,1},{17,25},{25,17},{2,10},{10... | collective-permute-start | bytes 393224 | tf_op jit(solution)/shard_map/ppermute | solution.py:29
  115.9 12.0 %all-to-all-start.5 = ((f32[16,2,128]{2,1,0:T(2,128)}), f32[16,2,128]{2,1,0:T(2,128)S(1)}, u32[]{:S(2)}, u32[]{:S(2)}) async-start(f32[16,2,128]{2,1,0:T(2,128)} %broadcast_in_dim.40), calls=%async_computation.5 | async-start | bytes 32768 | tf_op jit(solution)/shard_map/all_to_all | solution.py:21
  127.9 5.1 %collective-permute-start.13 = (bf16[128,512]{1,0:T(8,128)(2,1)S(1)}, bf16[128,512]{1,0:T(8,128)(2,1)S(1)}, u32[]{:S(2)}, u32[]{:S(2)}) collective-permute-start(bf16[128,512]{1,0:T(8,128)(2,1)S(1)} %get-tuple-element.35), channel_id=1, source_target_pairs={{0,2},{1,3},{2,0},{3,1},{4,6},{5,7},{6,4},{7,5},{8,10},{9,11},{10,... | collective-permute-start | bytes 393224 | tf_op jit(solution)/shard_map/ppermute | solution.py:29
  133.1 7.4 %all-to-all-done.5 = f32[16,2,128]{2,1,0:T(2,128)S(1)} async-done(((f32[16,2,128]{2,1,0:T(2,128)}), f32[16,2,128]{2,1,0:T(2,128)S(1)}, u32[]{:S(2)}, u32[]{:S(2)}) %all-to-all-start.5) | async-done | bytes 16416 | tf_op jit(solution)/shard_map/all_to_all | solution.py:21
  142.1 3.5 %collective-permute-start.12 = (bf16[128,1024]{1,0:T(8,128)(2,1)S(1)}, bf16[128,1024]{1,0:T(8,128)(2,1)S(1)}, u32[]{:S(2)}, u32[]{:S(2)}) collective-permute-start(bf16[128,1024]{1,0:T(8,128)(2,1)S(1)} %get-tuple-element.50), channel_id=1, source_target_pairs={{0,1},{1,0},{2,3},{3,2},{4,5},{5,4},{6,7},{7,6},{8,9},{9,8},{10,11... | collective-permute-start | bytes 786440 | tf_op jit(solution)/shard_map/ppermute | solution.py:29
  145.6 4.1 %collective-permute-start.15 = (bf16[128,1024]{1,0:T(8,128)(2,1)S(1)}, bf16[128,1024]{1,0:T(8,128)(2,1)S(1)}, u32[]{:S(2)}, u32[]{:S(2)}) collective-permute-start(bf16[128,1024]{1,0:T(8,128)(2,1)S(1)} %get-tuple-element.51), channel_id=1, source_target_pairs={{0,3},{1,2},{2,1},{3,0},{4,7},{5,6},{6,5},{7,4},{8,11},{9,10},{10,... | collective-permute-start | bytes 786440 | tf_op jit(solution)/shard_map/ppermute | solution.py:29
  150.0 2.6 %collective-permute-start.14 = (bf16[128,512]{1,0:T(8,128)(2,1)S(1)}, bf16[128,512]{1,0:T(8,128)(2,1)S(1)}, u32[]{:S(2)}, u32[]{:S(2)}) collective-permute-start(bf16[128,512]{1,0:T(8,128)(2,1)S(1)} %pad_maximum_fusion.4), channel_id=1, source_target_pairs={{0,2},{1,3},{2,0},{3,1},{4,6},{5,7},{6,4},{7,5},{8,10},{9,11},{10,... | collective-permute-start | bytes 393224 | tf_op jit(solution)/shard_map/ppermute | solution.py:29
  153.4 4.2 %all-to-all-start.6 = ((bf16[16,2,2048]{2,1,0:T(2,128)(2,1)}), bf16[16,2,2048]{2,1,0:T(2,128)(2,1)S(1)}, u32[]{:S(2)}, u32[]{:S(2)}) async-start(bf16[16,2,2048]{2,1,0:T(2,128)(2,1)} %reshape.282), calls=%async_computation.6 | async-start | bytes 262144 | tf_op jit(solution)/shard_map/all_to_all | solution.py:21
  158.6 1.9 %collective-permute-start.16 = (f32[512,256]{1,0:T(8,128)S(1)}, f32[512,256]{1,0:T(8,128)S(1)}, u32[]{:S(2)}, u32[]{:S(2)}) collective-permute-start(f32[512,256]{1,0:T(8,128)S(1)} %fusion.3), channel_id=1, source_target_pairs={{0,4},{4,0},{1,5},{5,1},{2,6},{6,2},{3,7},{7,3},{8,12},{12,8},{9,1... | collective-permute-start | bytes 1572872 | tf_op jit(solution)/shard_map/ppermute | solution.py:29
  161.3 9.4 %all-to-all-done.6 = bf16[16,2,2048]{2,1,0:T(2,128)(2,1)S(1)} async-done(((bf16[16,2,2048]{2,1,0:T(2,128)(2,1)}), bf16[16,2,2048]{2,1,0:T(2,128)(2,1)S(1)}, u32[]{:S(2)}, u32[]{:S(2)}) %all-to-all-start.6) | async-done | bytes 131104 | tf_op jit(solution)/shard_map/all_to_all | solution.py:21
  (128 shorter events, 27.4 us)
Async XLA Ops:
  3.9 15.3 %copy-start.3 = (bf16[5632,16]{0,1:T(8,128)(2,1)S(1)}, bf16[5632,16]{0,1:T(8,128)(2,1)}, u32[]{:S(2)}) copy-start(bf16[5632,16]{0,1:T(8,128)(2,1)} %param.10) | copy-start | bytes 540676
  3.9 39.1 %all-to-all-start = ((bf16[16,48,256]{2,1,0:T(8,128)(2,1)}), bf16[16,48,256]{2,1,0:T(8,128)(2,1)S(1)}, u32[]{:S(2)}, u32[]{:S(2)}) async-start(bf16[16,48,256]{2,1,0:T(8,128)(2,1)} %pad_add_fusion), calls=%async_computation | async-start | bytes 786432 | tf_op jit(solution)/shard_map/all_to_all | solution.py:21
  21.5 3.2 %collective-permute-start = (bf16[1,4,16,768]{3,2,1,0:T(8,128)(2,1)S(1)}, bf16[1,4,16,768]{3,2,1,0:T(8,128)(2,1)S(1)}, u32[]{:S(2)}, u32[]{:S(2)}) collective-permute-start(bf16[1,4,16,768]{3,2,1,0:T(8,128)(2,1)S(1)} %dynamic-slice_bitcast_fusion), channel_id=1, source_target_pairs={{0,4},{4,0},{1,5},{5,1},{2,6},{6,2},{3,7},{7,3},{8,12},{12,8},{9,1... | collective-permute-start | bytes 294920 | tf_op jit(solution)/shard_map/ppermute | solution.py:29
  23.5 21.3 %copy-start.1 = (bf16[2048,256]{1,0:T(8,128)(2,1)S(1)}, bf16[2048,256]{1,0:T(8,128)(2,1)}, u32[]{:S(2)}) copy-start(bf16[2048,256]{1,0:T(8,128)(2,1)} %param.12) | copy-start | bytes 3145732
  24.7 9.3 %collective-permute-start.1 = (bf16[1,2,16,768]{3,2,1,0:T(8,128)(2,1)S(1)}, bf16[1,2,16,768]{3,2,1,0:T(8,128)(2,1)S(1)}, u32[]{:S(2)}, u32[]{:S(2)}) collective-permute-start(bf16[1,2,16,768]{3,2,1,0:T(8,128)(2,1)S(1)} %get-tuple-element.48), channel_id=1, source_target_pairs={{0,8},{8,0},{16,24},{24,16},{1,9},{9,1},{17,25},{25,17},{2,10},{10... | collective-permute-start | bytes 147464 | tf_op jit(solution)/shard_map/ppermute | solution.py:29
  27.2 7.5 %collective-permute-start.2 = (bf16[1,2,16,768]{3,2,1,0:T(8,128)(2,1)S(1)}, bf16[1,2,16,768]{3,2,1,0:T(8,128)(2,1)S(1)}, u32[]{:S(2)}, u32[]{:S(2)}) collective-permute-start(bf16[1,2,16,768]{3,2,1,0:T(8,128)(2,1)S(1)} %get-tuple-element.49), channel_id=1, source_target_pairs={{0,16},{8,24},{16,0},{24,8},{1,17},{9,25},{17,1},{25,9},{2,18},{10... | collective-permute-start | bytes 147464 | tf_op jit(solution)/shard_map/ppermute | solution.py:29
  31.5 6.0 %collective-permute-start.3 = (bf16[1,2,16,768]{3,2,1,0:T(8,128)(2,1)S(1)}, bf16[1,2,16,768]{3,2,1,0:T(8,128)(2,1)S(1)}, u32[]{:S(2)}, u32[]{:S(2)}) collective-permute-start(bf16[1,2,16,768]{3,2,1,0:T(8,128)(2,1)S(1)} %get-tuple-element.47), channel_id=1, source_target_pairs={{0,24},{8,16},{16,8},{24,0},{1,25},{9,17},{17,9},{25,1},{2,26},{10... | collective-permute-start | bytes 147464 | tf_op jit(solution)/shard_map/ppermute | solution.py:29
  43.1 0.7 copy-start.2
  44.8 21.1 %collective-permute-start.4 = (bf16[2048,256]{1,0:T(8,128)(2,1)S(1)}, bf16[2048,256]{1,0:T(8,128)(2,1)S(1)}, u32[]{:S(2)}, u32[]{:S(2)}) collective-permute-start(bf16[2048,256]{1,0:T(8,128)(2,1)S(1)} %copy-done.1), channel_id=1, source_target_pairs={{0,4},{4,0},{1,5},{5,1},{2,6},{6,2},{3,7},{7,3},{8,12},{12,8},{9,1... | collective-permute-start | bytes 3145736 | tf_op jit(solution)/shard_map/ppermute | solution.py:29
  47.7 9.6 %all-to-all-start.1 = ((f32[8,32,128]{2,1,0:T(8,128)}), f32[8,32,128]{2,1,0:T(8,128)S(1)}, u32[]{:S(2)}, u32[]{:S(2)}) async-start(f32[8,32,128]{2,1,0:T(8,128)} %bitcast.14), calls=%async_computation.1 | async-start | bytes 262144 | tf_op jit(solution)/shard_map/all_to_all | solution.py:21
  58.0 22.3 %all-to-all-start.2 = ((bf16[16,32,128]{2,1,0:T(8,128)(2,1)}), bf16[16,32,128]{2,1,0:T(8,128)(2,1)S(1)}, u32[]{:S(2)}, u32[]{:S(2)}) async-start(bf16[16,32,128]{2,1,0:T(8,128)(2,1)} %broadcast_in_dim.35), calls=%async_computation.2 | async-start | bytes 262144 | tf_op jit(solution)/shard_map/all_to_all | solution.py:21
  66.4 13.9 %collective-permute-start.5 = (bf16[32,2048]{1,0:T(8,128)(2,1)S(1)}, bf16[32,2048]{1,0:T(8,128)(2,1)S(1)}, u32[]{:S(2)}, u32[]{:S(2)}) collective-permute-start(bf16[32,2048]{1,0:T(8,128)(2,1)S(1)} %get-tuple-element.43), channel_id=1, source_target_pairs={{0,8},{8,0},{16,24},{24,16},{1,9},{9,1},{17,25},{25,17},{2,10},{10... | collective-permute-start | bytes 393224 | tf_op jit(solution)/shard_map/ppermute | solution.py:29
  69.8 10.6 %collective-permute-start.6 = (bf16[32,2048]{1,0:T(8,128)(2,1)S(1)}, bf16[32,2048]{1,0:T(8,128)(2,1)S(1)}, u32[]{:S(2)}, u32[]{:S(2)}) collective-permute-start(bf16[32,2048]{1,0:T(8,128)(2,1)S(1)} %get-tuple-element.42), channel_id=1, source_target_pairs={{0,16},{8,24},{16,0},{24,8},{1,17},{9,25},{17,1},{25,9},{2,18},{10... | collective-permute-start | bytes 393224 | tf_op jit(solution)/shard_map/ppermute | solution.py:29
  71.9 8.6 %collective-permute-start.7 = (bf16[32,2048]{1,0:T(8,128)(2,1)S(1)}, bf16[32,2048]{1,0:T(8,128)(2,1)S(1)}, u32[]{:S(2)}, u32[]{:S(2)}) collective-permute-start(bf16[32,2048]{1,0:T(8,128)(2,1)S(1)} %get-tuple-element.41), channel_id=1, source_target_pairs={{0,24},{8,16},{16,8},{24,0},{1,25},{9,17},{17,9},{25,1},{2,26},{10... | collective-permute-start | bytes 393224 | tf_op jit(solution)/shard_map/ppermute | solution.py:29
  76.4 19.1 %collective-permute-start.8 = (f32[2,128]{1,0:T(2,128)S(1)}, f32[2,128]{1,0:T(2,128)S(1)}, u32[]{:S(2)}, u32[]{:S(2)}) collective-permute-start(f32[2,128]{1,0:T(2,128)S(1)} %bitcast.99), channel_id=1, source_target_pairs={{0,4},{4,0},{1,5},{5,1},{2,6},{6,2},{3,7},{7,3},{8,12},{12,8},{9,1... | collective-permute-start | bytes 3080 | tf_op jit(solution)/shard_map/ppermute | solution.py:29
  80.3 0.9 copy-start.6
  80.5 0.8 copy-start.8
  82.1 13.0 %all-to-all-start.3 = ((bf16[4,32,2048]{2,1,0:T(8,128)(2,1)}), bf16[4,32,2048]{2,1,0:T(8,128)(2,1)S(1)}, u32[]{:S(2)}, u32[]{:S(2)}) async-start(bf16[4,32,2048]{2,1,0:T(8,128)(2,1)} %broadcast_in_dim.37), calls=%async_computation.3 | async-start | bytes 1048576 | tf_op jit(solution)/shard_map/all_to_all | solution.py:21
  98.3 16.9 %all-to-all-start.4 = ((f32[4,2,128]{2,1,0:T(2,128)}), f32[4,2,128]{2,1,0:T(2,128)S(1)}, u32[]{:S(2)}, u32[]{:S(2)}) async-start(f32[4,2,128]{2,1,0:T(2,128)} %broadcast_in_dim.39), calls=%async_computation.4 | async-start | bytes 8192 | tf_op jit(solution)/shard_map/all_to_all | solution.py:21
  104.7 36.8 %collective-permute-start.10 = (bf16[32,2048]{1,0:T(8,128)(2,1)S(1)}, bf16[32,2048]{1,0:T(8,128)(2,1)S(1)}, u32[]{:S(2)}, u32[]{:S(2)}) collective-permute-start(bf16[32,2048]{1,0:T(8,128)(2,1)S(1)} %get-tuple-element.40), channel_id=1, source_target_pairs={{0,16},{8,24},{16,0},{24,8},{1,17},{9,25},{17,1},{25,9},{2,18},{10... | collective-permute-start | bytes 393224 | tf_op jit(solution)/shard_map/ppermute | solution.py:29
  108.7 32.8 %collective-permute-start.11 = (bf16[32,2048]{1,0:T(8,128)(2,1)S(1)}, bf16[32,2048]{1,0:T(8,128)(2,1)S(1)}, u32[]{:S(2)}, u32[]{:S(2)}) collective-permute-start(bf16[32,2048]{1,0:T(8,128)(2,1)S(1)} %get-tuple-element.39), channel_id=1, source_target_pairs={{0,24},{8,16},{16,8},{24,0},{1,25},{9,17},{17,9},{25,1},{2,26},{10... | collective-permute-start | bytes 393224 | tf_op jit(solution)/shard_map/ppermute | solution.py:29
  110.6 30.9 %collective-permute-start.9 = (bf16[32,2048]{1,0:T(8,128)(2,1)S(1)}, bf16[32,2048]{1,0:T(8,128)(2,1)S(1)}, u32[]{:S(2)}, u32[]{:S(2)}) collective-permute-start(bf16[32,2048]{1,0:T(8,128)(2,1)S(1)} %get-tuple-element.38), channel_id=1, source_target_pairs={{0,8},{8,0},{16,24},{24,16},{1,9},{9,1},{17,25},{25,17},{2,10},{10... | collective-permute-start | bytes 393224 | tf_op jit(solution)/shard_map/ppermute | solution.py:29
  115.9 24.6 %all-to-all-start.5 = ((f32[16,2,128]{2,1,0:T(2,128)}), f32[16,2,128]{2,1,0:T(2,128)S(1)}, u32[]{:S(2)}, u32[]{:S(2)}) async-start(f32[16,2,128]{2,1,0:T(2,128)} %broadcast_in_dim.40), calls=%async_computation.5 | async-start | bytes 32768 | tf_op jit(solution)/shard_map/all_to_all | solution.py:21
  127.9 30.2 %collective-permute-start.13 = (bf16[128,512]{1,0:T(8,128)(2,1)S(1)}, bf16[128,512]{1,0:T(8,128)(2,1)S(1)}, u32[]{:S(2)}, u32[]{:S(2)}) collective-permute-start(bf16[128,512]{1,0:T(8,128)(2,1)S(1)} %get-tuple-element.35), channel_id=1, source_target_pairs={{0,2},{1,3},{2,0},{3,1},{4,6},{5,7},{6,4},{7,5},{8,10},{9,11},{10,... | collective-permute-start | bytes 393224 | tf_op jit(solution)/shard_map/ppermute | solution.py:29
  140.5 1.0 copy-start.5
  140.5 1.0 copy-start.7
  140.5 1.0 copy-start.9
  142.1 15.5 %collective-permute-start.12 = (bf16[128,1024]{1,0:T(8,128)(2,1)S(1)}, bf16[128,1024]{1,0:T(8,128)(2,1)S(1)}, u32[]{:S(2)}, u32[]{:S(2)}) collective-permute-start(bf16[128,1024]{1,0:T(8,128)(2,1)S(1)} %get-tuple-element.50), channel_id=1, source_target_pairs={{0,1},{1,0},{2,3},{3,2},{4,5},{5,4},{6,7},{7,6},{8,9},{9,8},{10,11... | collective-permute-start | bytes 786440 | tf_op jit(solution)/shard_map/ppermute | solution.py:29
  145.6 12.3 %collective-permute-start.15 = (bf16[128,1024]{1,0:T(8,128)(2,1)S(1)}, bf16[128,1024]{1,0:T(8,128)(2,1)S(1)}, u32[]{:S(2)}, u32[]{:S(2)}) collective-permute-start(bf16[128,1024]{1,0:T(8,128)(2,1)S(1)} %get-tuple-element.51), channel_id=1, source_target_pairs={{0,3},{1,2},{2,1},{3,0},{4,7},{5,6},{6,5},{7,4},{8,11},{9,10},{10,... | collective-permute-start | bytes 786440 | tf_op jit(solution)/shard_map/ppermute | solution.py:29
  150.0 8.4 %collective-permute-start.14 = (bf16[128,512]{1,0:T(8,128)(2,1)S(1)}, bf16[128,512]{1,0:T(8,128)(2,1)S(1)}, u32[]{:S(2)}, u32[]{:S(2)}) collective-permute-start(bf16[128,512]{1,0:T(8,128)(2,1)S(1)} %pad_maximum_fusion.4), channel_id=1, source_target_pairs={{0,2},{1,3},{2,0},{3,1},{4,6},{5,7},{6,4},{7,5},{8,10},{9,11},{10,... | collective-permute-start | bytes 393224 | tf_op jit(solution)/shard_map/ppermute | solution.py:29
  153.4 17.3 %all-to-all-start.6 = ((bf16[16,2,2048]{2,1,0:T(2,128)(2,1)}), bf16[16,2,2048]{2,1,0:T(2,128)(2,1)S(1)}, u32[]{:S(2)}, u32[]{:S(2)}) async-start(bf16[16,2,2048]{2,1,0:T(2,128)(2,1)} %reshape.282), calls=%async_computation.6 | async-start | bytes 262144 | tf_op jit(solution)/shard_map/all_to_all | solution.py:21
  158.6 14.7 %collective-permute-start.16 = (f32[512,256]{1,0:T(8,128)S(1)}, f32[512,256]{1,0:T(8,128)S(1)}, u32[]{:S(2)}, u32[]{:S(2)}) collective-permute-start(f32[512,256]{1,0:T(8,128)S(1)} %fusion.3), channel_id=1, source_target_pairs={{0,4},{4,0},{1,5},{5,1},{2,6},{6,2},{3,7},{7,3},{8,12},{12,8},{9,1... | collective-permute-start | bytes 1572872 | tf_op jit(solution)/shard_map/ppermute | solution.py:29
  (6 other events, 4.2 us)
